TPU v7x, 32 devices: a whole 2x2x4 slice. The times are simulated.
32 devices in a mesh: ep: 8 (over z, y), tp: 4 (over x, core).
Axes of the slice: x: 2, y: 2, z: 4, core: 2. Of those that a mesh axis runs over, the one named last changes fastest.
Arguments:
- queries: bfloat16 [2048, 1536], P('ep', 'tp'), may hold values from -6 to 6
- kv_latent: bfloat16 [2048, 512], P('ep'), may hold values from -6 to 6
- rope_key: bfloat16 [2048, 64], P('ep'), may hold values from -6 to 6
- latent_gain: float32 [512], replicated, may hold values from 0.1 to 1.9
- w_key_up: bfloat16 [512, 1024], P(None, 'tp'), may hold values from -0.25 to 0.25
- w_value_up: bfloat16 [512, 1024], P(None, 'tp'), may hold values from -0.25 to 0.25
- query_gain: float32 [192], replicated, may hold values from 0.1 to 1.9
- key_gain: float32 [128], replicated, may hold values from 0.1 to 1.9
- rope_gain: float32 [64], replicated, may hold values from 0.1 to 1.9
- out_gain: float32 [128], replicated, may hold values from 0.1 to 1.9
- moe_tokens: bfloat16 [2048, 2048], P('ep'), may hold values from -6 to 6
- moe_gain: float32 [2048], replicated, may hold values from 0.1 to 1.9
- routes: int32 [2048, 2], P('ep'), may hold values from 0 to 7, all different within a row; in each aligned block of 64 rows (0 to 63, 64 to 127, ...) at most 24 rows name the same one
- route_weights: float32 [2048, 2], P('ep'), may hold values from 0.25 to 1
- w_gate: bfloat16 [8, 2048, 3584], P('ep', None, 'tp'), may hold values from -0.125 to 0.125
- w_up: bfloat16 [8, 2048, 3584], P('ep', None, 'tp'), may hold values from -0.125 to 0.125
- w_down: bfloat16 [8, 3584, 2048], P('ep', 'tp'), may hold values from -0.09375 to 0.09375
Outputs:
- attended: bfloat16 [2048, 1024], P('ep', 'tp')
- moe_out: bfloat16 [2048, 2048], P(('ep', 'tp'))
Inputs may be any that keep to these rules, and one draw needn't show every extreme that they name: `routes`: each row names 2 different experts of 0 to 7; in each aligned block of 64 rows no expert is named by more than 24 rows, and in some block one expert is named by exactly 24.
All inputs are finite; a program needn't handle non-finite values.
Results may differ from a plain program's by a relative error of at most 0.0071.
Values may be sent and summed in bfloat16 or wider, within the bound.
A program may use at most 128 MiB of HBM per device.

v0:
```python
import math

import jax
import jax.numpy as jnp
from jax import lax
from jax.sharding import PartitionSpec as P

EPS = 1e-06
THETA = 500000.0


def rms_norm(values, norm_gain):
    return values * lax.rsqrt(jnp.mean(values * values, axis=-1, keepdims=True) + EPS) * norm_gain


def rope_tables(positions, rope_dim):
    freqs = 1.0 / THETA ** (jnp.arange(0, rope_dim, 2, dtype=jnp.float32) / rope_dim)
    angles = positions.astype(jnp.float32)[:, None] * freqs[None, :]
    return (jnp.cos(angles), jnp.sin(angles))


def rotate(values, rot_cos, rot_sin):
    half_dim = values.shape[-1] // 2
    first_half = values[..., :half_dim]
    second_half = values[..., half_dim:]
    return jnp.concatenate(
        [
            first_half * rot_cos - second_half * rot_sin,
            second_half * rot_cos + first_half * rot_sin,
        ],
        axis=-1,
    )


def attention_part(
    queries,
    kv_latent,
    rope_key,
    latent_gain,
    w_key_up,
    w_value_up,
    query_gain,
    key_gain,
    rope_gain,
    out_gain,
):
    tok_rows = queries.shape[0]
    nope_dim = key_gain.shape[0]
    value_dim = out_gain.shape[0]
    rope_dim = rope_key.shape[1]
    head_count = w_key_up.shape[1] // nope_dim
    offset = lax.axis_index("ep") * tok_rows
    positions = offset + jnp.arange(tok_rows, dtype=jnp.int32)
    rot_cos, rot_sin = rope_tables(positions, rope_dim)
    latent = rms_norm(kv_latent.astype(jnp.float32), latent_gain).astype(jnp.bfloat16)
    key_nope = jnp.dot(latent, w_key_up, preferred_element_type=jnp.float32).reshape(
        tok_rows, head_count, nope_dim
    )
    key_nope = (
        rms_norm(key_nope, key_gain).astype(jnp.bfloat16).reshape(tok_rows, head_count * nope_dim)
    )
    values = jnp.dot(latent, w_value_up, preferred_element_type=jnp.float32).astype(jnp.bfloat16)
    rot_key = rotate(rms_norm(rope_key.astype(jnp.float32), rope_gain), rot_cos, rot_sin).astype(
        jnp.bfloat16
    )
    keys_values = jnp.concatenate([key_nope, values], axis=1)
    query = rms_norm(
        queries.astype(jnp.float32).reshape(tok_rows, head_count, nope_dim + rope_dim), query_gain
    )
    query_nope = query[..., :nope_dim].astype(jnp.bfloat16)
    query_rope = rotate(query[..., nope_dim:], rot_cos[:, None, :], rot_sin[:, None, :]).astype(
        jnp.bfloat16
    )
    scale = (nope_dim + rope_dim) ** (-0.5)
    last_pos = offset + tok_rows - 1
    initial = (
        jnp.zeros((tok_rows, head_count, value_dim), jnp.float32),
        jnp.zeros((head_count, tok_rows), jnp.float32),
    )
    totals = initial
    key_piece = lax.all_gather(keys_values, "ep", axis=0, tiled=True)
    rope_piece = lax.all_gather(rot_key, "ep", axis=0, tiled=True)
    piece_rows = key_piece.shape[0]
    block_rows = math.gcd(piece_rows, 512)

    def one_block(totals_in, block_index):
        block_first = block_index * block_rows
        kv_block = lax.dynamic_slice_in_dim(key_piece, block_first, block_rows, 0)
        rope_block = lax.dynamic_slice_in_dim(rope_piece, block_first, block_rows, 0)

        def attend(sums_in):
            weighted, denominator = sums_in
            key_block = kv_block[:, : head_count * nope_dim].reshape(
                block_rows, head_count, nope_dim
            )
            value_block = kv_block[:, head_count * nope_dim :].reshape(
                block_rows, head_count, value_dim
            )
            scores = (
                jnp.einsum(
                    "qhd,khd->hqk", query_nope, key_block, preferred_element_type=jnp.float32
                )
                + jnp.einsum(
                    "qhr,kr->hqk", query_rope, rope_block, preferred_element_type=jnp.float32
                )
            ) * scale
            key_pos = block_first + jnp.arange(block_rows, dtype=jnp.int32)
            visible = (positions[:, None] >= key_pos[None, :])[None]
            exp_scores = jnp.where(visible, jnp.exp(scores), 0.0)
            denominator = denominator + jnp.sum(exp_scores, axis=-1)
            weighted = weighted + jnp.einsum(
                "hqk,khd->qhd",
                exp_scores.astype(jnp.bfloat16),
                value_block,
                preferred_element_type=jnp.float32,
            )
            return (weighted, denominator)

        def unchanged(sums_in):
            return sums_in

        return (lax.cond(block_first <= last_pos, attend, unchanged, totals_in), None)

    totals, _ = lax.scan(one_block, totals, jnp.arange(piece_rows // block_rows, dtype=jnp.int32))
    weighted, denominator = totals
    mixed = weighted / jnp.transpose(denominator)[:, :, None]
    return rms_norm(mixed, out_gain).astype(jnp.bfloat16).reshape(tok_rows, head_count * value_dim)


def experts_part(moe_tokens, moe_gain, routes, route_weights, w_gate, w_up, w_down):
    n_rows = moe_tokens.shape[0]
    model_dim = moe_tokens.shape[1]
    top_count = routes.shape[1]
    quarters = lax.axis_size("tp")
    part_rows = n_rows // quarters
    experts = lax.axis_size("ep") * w_gate.shape[0]
    capacity = (3 * top_count * part_rows + 2 * experts - 1) // (2 * experts)
    slot_count = experts * capacity
    normed = rms_norm(moe_tokens.astype(jnp.float32), moe_gain).astype(jnp.bfloat16)
    chosen = routes.reshape(quarters, part_rows * top_count)
    onehot = (chosen[..., None] == jnp.arange(experts, dtype=jnp.int32)).astype(jnp.int32)
    rank = jnp.sum((jnp.cumsum(onehot, axis=1) - onehot) * onehot, axis=-1)
    slots = chosen * capacity + rank
    slot_hit = (slots[..., None] == jnp.arange(slot_count, dtype=jnp.int32)).astype(jnp.bfloat16)
    slot_hit = slot_hit.reshape(quarters, part_rows, top_count, slot_count)
    my_part = lax.axis_index("tp")
    mine_hit = lax.dynamic_index_in_dim(slot_hit, my_part, 0, keepdims=False)
    down_cols = w_down[0]
    own_rows = lax.dynamic_slice_in_dim(normed, my_part * part_rows, part_rows, 0)
    outgoing = jnp.einsum(
        "rs,rd->sd", jnp.sum(mine_hit, axis=1), own_rows, preferred_element_type=jnp.float32
    )
    outgoing = outgoing.astype(jnp.bfloat16).reshape(1, experts, capacity, model_dim)
    arrived = lax.all_gather(
        lax.all_to_all(outgoing, "ep", split_axis=1, concat_axis=1, tiled=True),
        "tp",
        axis=0,
        tiled=True,
    )
    gate = jnp.einsum("abcd,df->abcf", arrived, w_gate[0], preferred_element_type=jnp.float32)
    upward = jnp.einsum("abcd,df->abcf", arrived, w_up[0], preferred_element_type=jnp.float32)
    hidden = (jax.nn.silu(gate) * upward).astype(jnp.bfloat16)
    summed = lax.psum_scatter(
        jnp.einsum("abcf,fd->abcd", hidden, down_cols, preferred_element_type=jnp.float32),
        "tp",
        scatter_dimension=0,
        tiled=True,
    ).astype(jnp.bfloat16)
    returned = lax.all_to_all(summed, "ep", split_axis=1, concat_axis=1, tiled=True)
    picked = jnp.einsum(
        "rks,sd->rkd",
        mine_hit,
        returned.reshape(slot_count, model_dim),
        preferred_element_type=jnp.float32,
    )
    own_weights = lax.dynamic_slice_in_dim(route_weights, my_part * part_rows, part_rows, 0)
    return jnp.sum(picked * own_weights[:, :, None], axis=1).astype(jnp.bfloat16)


def on_device(
    queries,
    kv_latent,
    rope_key,
    latent_gain,
    w_key_up,
    w_value_up,
    query_gain,
    key_gain,
    rope_gain,
    out_gain,
    moe_tokens,
    moe_gain,
    routes,
    route_weights,
    w_gate,
    w_up,
    w_down,
):
    attended = attention_part(
        queries,
        kv_latent,
        rope_key,
        latent_gain,
        w_key_up,
        w_value_up,
        query_gain,
        key_gain,
        rope_gain,
        out_gain,
    )
    moe_out = experts_part(moe_tokens, moe_gain, routes, route_weights, w_gate, w_up, w_down)
    return (attended, moe_out)


def solution(mesh):
    return jax.shard_map(
        on_device,
        mesh=mesh,
        in_specs=(
            P("ep", "tp"),
            P("ep", None),
            P("ep", None),
            P(),
            P(None, "tp"),
            P(None, "tp"),
            P(),
            P(),
            P(),
            P(),
            P("ep", None),
            P(),
            P("ep", None),
            P("ep", None),
            P("ep", None, "tp"),
            P("ep", None, "tp"),
            P("ep", "tp", None),
        ),
        out_specs=(P("ep", "tp"), P(("ep", "tp"), None)),
        check_vma=False,
    )
```

profile of v0, /device:TPU:24, one launch (start us, length us, event | category | flops | bytes accessed | tf_op | source)
XLA Modules:
  0.0 215.2 jit_solution(17338202645033800728)
XLA Ops:
  8.1 0.8 copy.48
  8.9 0.7 broadcast_multiply_fusion
  9.6 1.5 multiply_reduce_fusion
  11.1 1.5 convert_element_type.75
  14.4 23.4 %all_to_all.10 = bf16[1,8,24,2048]{3,2,0,1:T(8,128)(2,1)} all-to-all(bf16[1,8,24,2048]{3,2,0,1:T(8,128)(2,1)S(1)} %bitcast.98), channel_id=1, replica_groups=mesh['ep'=8,'tp'=4] {'ep'}, dimensions={1} | all-to-all | bytes 1572864 | tf_op jit(solution)/shard_map/all_to_all | solution.py:155
  37.9 29.8 %all-gather.5.cloned.1.call-done = bf16[4,8,24,2048]{3,2,1,0:T(8,128)(2,1)} async-done(((bf16[1,8,24,2048]{3,2,1,0:T(8,128)(2,1)}), bf16[4,8,24,2048]{3,2,1,0:T(8,128)(2,1)}) %all-gather.5.cloned.1.call-update) | async-done | bytes 3145744 | tf_op jit(solution)/shard_map/all_gather | solution.py:154
  67.7 6.5 %fusion.13 = f32[4,8,24,896]{3,2,1,0:T(8,128)S(1)} fusion(bf16[4,8,24,2048]{3,2,1,0:T(8,128)(2,1)} %all-gather.5.cloned.1.call-done, bf16[1,2048,896]{2,1,0:T(8,128)(2,1)} %param.36), kind=kOutput, calls=%fused_computation.19 | convolution fusion | flops 2818572288 | bytes 9568256 | tf_op jit(solution)/shard_map/abcd,df->abcf/dot_general | solution.py:161
  74.3 3.7 %multiply_convert_fusion = bf16[4,8,24,896]{3,2,1,0:T(8,128)(2,1)S(1)} fusion(f32[4,8,24,896]{3,2,1,0:T(8,128)S(1)} %fusion.13, bf16[4,8,24,2048]{3,2,1,0:T(8,128)(2,1)S(1)} %copy-done.11, bf16[1,2048,896]{2,1,0:T(8,128)(2,1)S(1)} %copy-done.9), kind=kOutput, calls=%fused_computation.23 | convolution fusion | flops 2822701056 | bytes 10944512 | tf_op jit(solution)/shard_map/abcd,df->abcf/dot_general | solution.py:160
  78.1 5.3 %fusion.11 = f32[4,8,24,2048]{3,2,1,0:T(8,128)} fusion(bf16[4,8,24,896]{3,2,1,0:T(8,128)(2,1)S(1)} %multiply_convert_fusion, bf16[1,896,2048]{2,1,0:T(8,128)(2,1)S(1)} %copy-done.10), kind=kOutput, calls=%fused_computation.17 | convolution fusion | flops 2818572288 | bytes 11337728 | tf_op jit(solution)/shard_map/abcf,fd->abcd/dot_general | solution.py:164
  83.5 0.8 copy-done.1
  85.3 0.7 pad_maximum_fusion
  86.8 55.6 %reduce-scatter.2.cloned.1.call-done = f32[1,8,24,2048]{3,2,1,0:T(8,128)} async-done(((f32[4,8,24,2048]{3,2,1,0:T(8,128)}), f32[1,8,24,2048]{3,2,1,0:T(8,128)}) %reduce-scatter.2.cloned.1.call-update) | async-done | bytes 1572880 | tf_op jit(solution)/shard_map/reduce_scatter | solution.py:163
  142.4 2.4 %convert_bitcast_fusion = bf16[1,8,24,2048]{3,2,0,1:T(8,128)(2,1)} fusion(f32[1,8,24,2048]{3,2,1,0:T(8,128)} %reduce-scatter.2.cloned.1.call-done), kind=kLoop, calls=%fused_computation.29 | loop fusion | flops 393216 | bytes 2359296 | tf_op jit(solution)/shard_map/convert_element_type | solution.py:168
  144.8 6.0 %all-to-all-start.1 = ((bf16[1,8,24,2048]{3,2,0,1:T(8,128)(2,1)}), bf16[1,8,24,2048]{3,2,0,1:T(8,128)(2,1)S(1)}, u32[]{:S(2)}, u32[]{:S(2)}) async-start(bf16[1,8,24,2048]{3,2,0,1:T(8,128)(2,1)} %convert_bitcast_fusion), calls=%async_computation.2 | async-start | bytes 1572864 | tf_op jit(solution)/shard_map/all_to_all | solution.py:169
  151.1 38.3 %all_gather.10 = bf16[2048,64]{0,1:T(8,128)(2,1)S(1)} all-gather(bf16[256,64]{0,1:T(8,128)(2,1)S(1)} %pad_maximum_fusion.2), channel_id=1, replica_groups=mesh['ep'=8,'tp'=4] {'ep'}, dimensions={0}, use_global_device_ids=true | all-gather | bytes 294912 | tf_op jit(solution)/shard_map/all_gather | solution.py:82
  189.4 16.3 %while.13 = (s32[]{:T(128)}, f32[256,2,128]{2,0,1:T(8,128)S(1)}, f32[2,256]{1,0:T(2,128)S(1)}, s32[4]{0:T(128)S(1)}, s32[]{:T(128)}, /*index=5*/bf16[2048,512]{0...) while((s32[]{:T(128)}, f32[256,2,128]{2,0,1:T(8,128)S(1)}, ...), condition=%wide.region_8.9_spmd.clone, body=%wide.region_4.8_spmd.clone.sunk | while | flops 169280256 | bytes 5783885 | solution.py:124
  189.4 0.6 dynamic_slice.62
  190.6 2.8 %conditional.3 = ((f32[256,2,128]{2,0,1:T(8,128)S(1)}, f32[2,256]{1,0:T(2,128)S(1)})) conditional(s32[]{:T(128)} %convert_element_type.127, (f32[256,2,128]{2,0,1:T(8,128)S(1)}, f32[2,256]{1,0:T(2,128)S(1)}) %tuple.58, (s32[]{:T(128)}, s32[]{:T(128)}, bf16[2048,512]{0,1:T(8,128)(2,1)}, bf16[256,2,128]{2,0,1:T(8,128)(2,1)S(1)}, ...), branch_computations={%region_5.5_spmd, %region_6.7_spmd} | conditional | flops 169280256 | bytes 5782618 | solution.py:122
  190.7 1.3 constant_dynamic-slice_fusion
  192.5 0.5 fusion.42
  193.5 0.6 dynamic_slice.62
  194.7 2.8 %conditional.3 = ((f32[256,2,128]{2,0,1:T(8,128)S(1)}, f32[2,256]{1,0:T(2,128)S(1)})) conditional(s32[]{:T(128)} %convert_element_type.127, (f32[256,2,128]{2,0,1:T(8,128)S(1)}, f32[2,256]{1,0:T(2,128)S(1)}) %tuple.58, (s32[]{:T(128)}, s32[]{:T(128)}, bf16[2048,512]{0,1:T(8,128)(2,1)}, bf16[256,2,128]{2,0,1:T(8,128)(2,1)S(1)}, ...), branch_computations={%region_5.5_spmd, %region_6.7_spmd} | conditional | flops 169280256 | bytes 5782618 | solution.py:122
  194.8 1.3 constant_dynamic-slice_fusion
  196.6 0.5 fusion.42
  197.6 0.6 dynamic_slice.62
  198.8 2.8 %conditional.3 = ((f32[256,2,128]{2,0,1:T(8,128)S(1)}, f32[2,256]{1,0:T(2,128)S(1)})) conditional(s32[]{:T(128)} %convert_element_type.127, (f32[256,2,128]{2,0,1:T(8,128)S(1)}, f32[2,256]{1,0:T(2,128)S(1)}) %tuple.58, (s32[]{:T(128)}, s32[]{:T(128)}, bf16[2048,512]{0,1:T(8,128)(2,1)}, bf16[256,2,128]{2,0,1:T(8,128)(2,1)S(1)}, ...), branch_computations={%region_5.5_spmd, %region_6.7_spmd} | conditional | flops 169280256 | bytes 5782618 | solution.py:122
  198.8 1.3 constant_dynamic-slice_fusion
  201.6 0.6 dynamic_slice.62
  202.9 2.7 %conditional.3 = ((f32[256,2,128]{2,0,1:T(8,128)S(1)}, f32[2,256]{1,0:T(2,128)S(1)})) conditional(s32[]{:T(128)} %convert_element_type.127, (f32[256,2,128]{2,0,1:T(8,128)S(1)}, f32[2,256]{1,0:T(2,128)S(1)}) %tuple.58, (s32[]{:T(128)}, s32[]{:T(128)}, bf16[2048,512]{0,1:T(8,128)(2,1)}, bf16[256,2,128]{2,0,1:T(8,128)(2,1)S(1)}, ...), branch_computations={%region_5.5_spmd, %region_6.7_spmd} | conditional | flops 169280256 | bytes 5782618 | solution.py:122
  202.9 1.3 constant_dynamic-slice_fusion
  205.9 0.9 copy_bitcast_fusion
  206.8 1.0 fusion.19
  (109 shorter events, 8.7 us)
Async XLA Ops:
  8.0 76.5 %copy-start = (bf16[512,256]{1,0:T(8,128)(2,1)S(1)}, bf16[512,256]{1,0:T(8,128)(2,1)}, u32[]{:S(2)}) copy-start(bf16[512,256]{1,0:T(8,128)(2,1)} %param.25) | copy-start | bytes 786436
  8.0 59.7 %all-gather.5.cloned.1.call-start = ((), (), s32[]{:S(2)}) async-start(), calls=%async_computation.4 | async-start | bytes 3932160 | tf_op jit(solution)/shard_map/all_gather | solution.py:154
  9.6 4.4 %copy-start.4 = (f32[2048]{0:T(1024)S(1)}, f32[2048]{0:T(1024)}, u32[]{:S(2)}) copy-start(f32[2048]{0:T(1024)} %param.32) | copy-start | bytes 24580
  37.8 104.5 %reduce-scatter.2.cloned.1.call-start = ((), (), s32[]{:S(2)}) async-start(), calls=%async_computation.5 | async-start | bytes 7864320 | tf_op jit(solution)/shard_map/reduce_scatter | solution.py:163
  67.7 6.6 %copy-start.9 = (bf16[1,2048,896]{2,1,0:T(8,128)(2,1)S(1)}, bf16[1,2048,896]{2,1,0:T(8,128)(2,1)}, u32[]{:S(2)}) copy-start(bf16[1,2048,896]{2,1,0:T(8,128)(2,1)} %param.35) | copy-start | bytes 11010052
  67.7 6.6 %copy-start.11 = (bf16[4,8,24,2048]{3,2,1,0:T(8,128)(2,1)S(1)}, bf16[4,8,24,2048]{3,2,1,0:T(8,128)(2,1)}, u32[]{:S(2)}) copy-start(bf16[4,8,24,2048]{3,2,1,0:T(8,128)(2,1)} %all-gather.5.cloned.1.call-done) | copy-start | bytes 9437188
  74.3 3.8 %copy-start.10 = (bf16[1,896,2048]{2,1,0:T(8,128)(2,1)S(1)}, bf16[1,896,2048]{2,1,0:T(8,128)(2,1)}, u32[]{:S(2)}) copy-start(bf16[1,896,2048]{2,1,0:T(8,128)(2,1)} %param.37) | copy-start | bytes 11010052
  83.4 0.9 copy-start.1
  83.4 1.1 copy-start.14
  83.4 1.1 copy-start.13
  83.4 1.6 copy-start.12
  83.4 2.7 %copy-start.2 = (bf16[256,384]{1,0:T(8,128)(2,1)S(1)}, bf16[256,384]{1,0:T(8,128)(2,1)}, u32[]{:S(2)}) copy-start(bf16[256,384]{1,0:T(8,128)(2,1)} %param.21) | copy-start | bytes 589828
  83.4 2.9 %copy-start.5 = (f32[192]{0:T(256)S(1)}, f32[192]{0:T(256)}, u32[]{:S(2)}) copy-start(f32[192]{0:T(256)} %param.27) | copy-start | bytes 2308
  83.4 3.2 %copy-start.8 = (f32[256,2]{0,1:T(2,128)S(1)}, f32[256,2]{0,1:T(2,128)}, u32[]{:S(2)}) copy-start(f32[256,2]{0,1:T(2,128)} %param.34) | copy-start | bytes 6148
  83.4 3.3 %copy-start.3 = (bf16[256,64]{0,1:T(8,128)(2,1)S(1)}, bf16[256,64]{0,1:T(8,128)(2,1)}, u32[]{:S(2)}) copy-start(bf16[256,64]{0,1:T(8,128)(2,1)} %param.23) | copy-start | bytes 98308
  83.4 3.3 %copy-start.6 = (f32[64]{0:T(128)S(1)}, f32[64]{0:T(128)}, u32[]{:S(2)}) copy-start(f32[64]{0:T(128)} %param.29) | copy-start | bytes 772
  83.4 105.9 %all-gather.3.cloned.1.call-start = ((), (), s32[]{:S(2)}) async-start(), calls=%async_computation.3 | async-start | bytes 2359296 | tf_op jit(solution)/shard_map/all_gather | solution.py:81
  144.8 62.0 %all-to-all-start.1 = ((bf16[1,8,24,2048]{3,2,0,1:T(8,128)(2,1)}), bf16[1,8,24,2048]{3,2,0,1:T(8,128)(2,1)S(1)}, u32[]{:S(2)}, u32[]{:S(2)}) async-start(bf16[1,8,24,2048]{3,2,0,1:T(8,128)(2,1)} %convert_bitcast_fusion), calls=%async_computation.2 | async-start | bytes 1572864 | tf_op jit(solution)/shard_map/all_to_all | solution.py:169
  189.4 16.5 %copy-start.7 = (f32[128]{0:T(128)S(1)}, f32[128]{0:T(128)}, u32[]{:S(2)}) copy-start(f32[128]{0:T(128)} %param.30) | copy-start | bytes 1540
Sparse Core Ops, SparseCore 0:
  38.0 29.6 all-gather.4
  83.5 58.8 reduce-scatter.1
Sparse Core Ops, SparseCore 1:
  86.5 48.5 all-gather.2
where the time goes:
time: 216 us; the launch traced here: 215 us
  waiting for transfers between devices  85.4 us (40%)
  blocking collectives  61.7 us (29%)
  matrix products  22.6 us (10%)
  between operations  15.9 us (7%)
  local copies, waits for them, and re-layouts  10.3 us (5%)
  other arithmetic  10.1 us (5%)
  starting transfers between devices  6.13 us (3%)
  loops' own time  3.02 us (1%)
    reduce_scatter x1, waiting for transfers between devices, experts_part(): lax.psum_scatter(jnp.einsum('abcf,fd->abcd', hidden, down_cols, preferred...  55.6 us
    all_gather x1, blocking collectives, attention_part(): rope_piece = lax.all_gather(rot_key, 'ep', axis=0, tiled=True)  38.3 us
    all_gather x1, waiting for transfers between devices, experts_part(): lax.all_gather(lax.all_to_all(outgoing, 'ep', split_axis=1, concat_axis=1...  29.8 us
    all_to_all x1, blocking collectives, experts_part(): lax.all_to_all(outgoing, 'ep', split_axis=1, concat_axis=1, tiled=True)  23.4 us
    dot_general x1, matrix products, experts_part(): jnp.einsum('abcd,df->abcf', arrived, w_up[0], preferred_element_type=jnp....  6.55 us
    all_to_all x1, starting transfers between devices, experts_part(): lax.all_to_all(summed, 'ep', split_axis=1, concat_axis=1, tiled=True)  6.01 us
    slice x4, local copies, waits for them, and re-layouts, attend(): kv_block[:, :head_count * nope_dim]  5.31 us
    dot_general x1, matrix products, experts_part(): jnp.einsum('abcf,fd->abcd', hidden, down_cols, preferred_element_type=jnp...  5.3 us
  transfers between devices with their start and end apart: 4, of which 2 were waited for; matrix products, arithmetic and copies ran while one was open for 9% of the time, Pallas kernels for 0%

commit v1 on v0

v1 whole, which is shorter than its diff:
```python
import functools
import math

import jax
import jax.numpy as jnp
from jax import lax
from jax.experimental import pallas as pl
from jax.experimental.pallas import tpu as pltpu
from jax.sharding import PartitionSpec as P

EPS = 1e-06
THETA = 500000.0


def rms_norm(values, norm_gain):
    return values * lax.rsqrt(jnp.mean(values * values, axis=-1, keepdims=True) + EPS) * norm_gain


def rope_tables(positions, rope_dim):
    freqs = 1.0 / THETA ** (jnp.arange(0, rope_dim, 2, dtype=jnp.float32) / rope_dim)
    angles = positions.astype(jnp.float32)[:, None] * freqs[None, :]
    return (jnp.cos(angles), jnp.sin(angles))


def rotate(values, rot_cos, rot_sin):
    half_dim = values.shape[-1] // 2
    first_half = values[..., :half_dim]
    second_half = values[..., half_dim:]
    return jnp.concatenate(
        [
            first_half * rot_cos - second_half * rot_sin,
            second_half * rot_cos + first_half * rot_sin,
        ],
        axis=-1,
    )

MESH = pl.DeviceIdType.MESH
VMEM = pltpu.VMEM


def remote(src, dst, send, recv, device):
    return pltpu.make_async_remote_copy(
        src_ref=src, dst_ref=dst, send_sem=send, recv_sem=recv, device_id=device, device_id_type=MESH
    )


def greet(me, quarter, n_ep, highs):
    high, low = quarter // 2, quarter % 2
    barrier = pltpu.get_barrier_semaphore()

    def hello(device):
        pl.semaphore_signal(barrier, inc=1, device_id=device, device_id_type=MESH)

    def hello_ep(step, carry):
        hello((lax.rem(me + step, n_ep), quarter))
        return carry

    lax.fori_loop(1, n_ep, hello_ep, 0)
    hello((me, high * 2 + 1 - low))
    for step in range(1, highs):
        hello((me, lax.rem(high + step, highs) * 2 + low))
    pl.semaphore_wait(barrier, n_ep - 1 + 1 + highs - 1)


def spread_kernel(
    n_ep, highs, rows_ref, lat_ref, arrived, lat_all,
    own_sem, ep_send, ep_recv, high_send, high_recv, low_send, low_recv,
):
    me, quarter = lax.axis_index("ep"), lax.axis_index("tp")
    high, low = quarter // 2, quarter % 2
    partner = (me, high * 2 + 1 - low)
    greet(me, quarter, n_ep, highs)
    payloads = (
        (lambda j: rows_ref.at[j], arrived),
        (lambda j: lat_ref, lat_all),
    )
    own = [
        pltpu.make_async_copy(outgoing(me), into.at[low, high, me], own_sem.at[p])
        for p, (outgoing, into) in enumerate(payloads)
    ]
    for copy in own:
        copy.start()

    def ep_copy(p, step):
        outgoing, into = payloads[p]
        j = lax.rem(me + step, n_ep)
        return remote(
            outgoing(j), into.at[low, high, me], ep_send.at[p, step], ep_recv.at[p, step], (j, quarter)
        )

    def ep_arrival(p, step):
        outgoing, into = payloads[p]
        j = lax.rem(me + n_ep - step, n_ep)
        return remote(
            outgoing(me), into.at[low, high, j], ep_send.at[p, step], ep_recv.at[p, step], (j, quarter)
        )

    def high_copy(p, step, hop):
        into = payloads[p][1]
        j = lax.rem(me + n_ep - step, n_ep)
        block = into.at[low, high, j]
        return remote(
            block, block, high_send.at[p, hop, step], high_recv.at[p, hop, step],
            (me, lax.rem(high + hop, highs) * 2 + low),
        )

    def high_arrival(p, step, hop):
        into = payloads[p][1]
        j = lax.rem(me + n_ep - step, n_ep)
        block = into.at[low, lax.rem(high + highs - hop, highs), j]
        return remote(
            block, block, high_send.at[p, hop, step], high_recv.at[p, hop, step],
            (me, lax.rem(high + hop, highs) * 2 + low),
        )

    def low_copy(p, step, hop, side):
        into = payloads[p][1]
        j = lax.rem(me + n_ep - step, n_ep)
        block = into.at[side, lax.rem(high + highs - hop, highs), j]
        return remote(block, block, low_send.at[p, hop, step], low_recv.at[p, hop, step], partner)

    def start_ep(step, carry, p):
        ep_copy(p, step).start()
        return carry

    def forward(step, carry, p):
        ep_arrival(p, step).wait_recv()
        for hop in range(1, highs):
            high_copy(p, step, hop).start()
        low_copy(p, step, 0, low).start()
        return carry

    def forward_low(step, carry, p):
        for hop in range(1, highs):
            high_arrival(p, step, hop).wait_recv()
            low_copy(p, step, hop, low).start()
        return carry

    def finish(step, carry, p):
        for hop in range(highs):
            low_copy(p, step, hop, 1 - low).wait_recv()
            low_copy(p, step, hop, low).wait_send()
        for hop in range(1, highs):
            high_copy(p, step, hop).wait_send()
        return carry

    def finish_ep(step, carry, p):
        ep_copy(p, step).wait_send()
        return carry

    for p in range(2):
        lax.fori_loop(1, n_ep, functools.partial(start_ep, p=p), 0)
    for p in range(2):
        own[p].wait()
        for hop in range(1, highs):
            high_copy(p, 0, hop).start()
        low_copy(p, 0, 0, low).start()
        lax.fori_loop(1, n_ep, functools.partial(forward, p=p), 0)
    for p in range(2):
        lax.fori_loop(0, n_ep, functools.partial(forward_low, p=p), 0)
    for p in range(2):
        lax.fori_loop(0, n_ep, functools.partial(finish, p=p), 0)
        lax.fori_loop(1, n_ep, functools.partial(finish_ep, p=p), 0)


def spread(rows, lat, quarters):
    n_ep, cap, model_dim = rows.shape
    highs = quarters // 2
    dma = pltpu.SemaphoreType.DMA
    return pl.pallas_call(
        functools.partial(spread_kernel, n_ep, highs),
        out_shape=(
            jax.ShapeDtypeStruct((2, highs, n_ep, cap, model_dim), rows.dtype),
            jax.ShapeDtypeStruct((2, highs, n_ep) + lat.shape, lat.dtype),
        ),
        in_specs=[pl.BlockSpec(memory_space=VMEM)] * 2,
        out_specs=(pl.BlockSpec(memory_space=VMEM),) * 2,
        scratch_shapes=[
            dma((2,)),
            dma((2, n_ep)),
            dma((2, n_ep)),
            dma((2, highs, n_ep)),
            dma((2, highs, n_ep)),
            dma((2, highs, n_ep)),
            dma((2, highs, n_ep)),
        ],
        compiler_params=pltpu.CompilerParams(
            collective_id=0, has_side_effects=True, vmem_limit_bytes=60 << 20
        ),
        name="spread",
    )(rows, lat)


def collect_kernel(
    n_ep, highs, part_ref, ret, low_buf, high_buf, sum_buf, final_buf,
    low_send, low_recv, high_send, high_recv, ep_send, ep_recv,
):
    me, quarter = lax.axis_index("ep"), lax.axis_index("tp")
    high, low = quarter // 2, quarter % 2
    partner = (me, high * 2 + 1 - low)
    greet(me, quarter, n_ep, highs)

    def low_copy(step):
        j = lax.rem(me + step, n_ep)
        return remote(
            part_ref.at[1 - low, j], low_buf.at[j], low_send.at[step], low_recv.at[step], partner
        )

    def high_copy(step, hop):
        j = lax.rem(me + step, n_ep)
        other = lax.rem(high + hop, highs)
        return remote(
            sum_buf.at[j, other], high_buf.at[hop, j], high_send.at[hop, step],
            high_recv.at[hop, step], (me, other * 2 + low),
        )

    def ep_copy(step):
        j = lax.rem(me + step, n_ep)
        return remote(final_buf.at[j], ret.at[me], ep_send.at[step], ep_recv.at[step], (j, quarter))

    def ep_arrival(step):
        j = lax.rem(me + n_ep - step, n_ep)
        return remote(final_buf.at[j], ret.at[j], ep_send.at[step], ep_recv.at[step], (j, quarter))

    def start_low(step, carry):
        low_copy(step).start()
        return carry

    def add_low(step, carry):
        low_copy(step).wait_recv()
        j = lax.rem(me + step, n_ep)
        sum_buf[j] = (
            part_ref[low, j].astype(jnp.float32) + low_buf[j].astype(jnp.float32)
        ).astype(jnp.bfloat16)
        for hop in range(1, highs):
            high_copy(step, hop).start()
        return carry

    def total(step):
        j = lax.rem(me + step, n_ep)
        value = part_ref[low, j, high].astype(jnp.float32) + low_buf[j, high].astype(jnp.float32)
        for hop in range(1, highs):
            high_copy(step, hop).wait_recv()
            value = value + high_buf[hop, j].astype(jnp.float32)
        return value.astype(jnp.bfloat16)

    def add_high(step, carry):
        final_buf[lax.rem(me + step, n_ep)] = total(step)
        ep_copy(step).start()
        return carry

    def finish(step, carry):
        ep_arrival(step).wait_recv()
        ep_copy(step).wait_send()
        return carry

    def finish_tp(step, carry):
        low_copy(step).wait_send()
        for hop in range(1, highs):
            high_copy(step, hop).wait_send()
        return carry

    lax.fori_loop(1, n_ep, start_low, 0)
    low_copy(0).start()
    lax.fori_loop(1, n_ep, add_low, 0)
    add_low(0, 0)
    lax.fori_loop(1, n_ep, add_high, 0)
    ret[me] = total(0)
    lax.fori_loop(1, n_ep, finish, 0)
    lax.fori_loop(0, n_ep, finish_tp, 0)


def collect(partial):
    _, n_ep, highs, cap, model_dim = partial.shape
    dma = pltpu.SemaphoreType.DMA
    kind = partial.dtype
    return pl.pallas_call(
        functools.partial(collect_kernel, n_ep, highs),
        out_shape=jax.ShapeDtypeStruct((n_ep, cap, model_dim), kind),
        in_specs=[pl.BlockSpec(memory_space=VMEM)],
        out_specs=pl.BlockSpec(memory_space=VMEM),
        scratch_shapes=[
            VMEM((n_ep, highs, cap, model_dim), kind),
            VMEM((highs, n_ep, cap, model_dim), kind),
            VMEM((n_ep, highs, cap, model_dim), kind),
            VMEM((n_ep, cap, model_dim), kind),
            dma((n_ep,)),
            dma((n_ep,)),
            dma((highs, n_ep)),
            dma((highs, n_ep)),
            dma((n_ep,)),
            dma((n_ep,)),
        ],
        compiler_params=pltpu.CompilerParams(
            collective_id=1, has_side_effects=True, vmem_limit_bytes=62 << 20
        ),
        name="collect",
    )(partial)


def attend_kernel(
    heads, nope_dim, value_dim, latent_dim, scale,
    lat_ref, wk_ref, wv_ref, qn_ref, qr_ref, kg_ref, og_ref, out_ref, acc, den,
):
    block = pl.program_id(0)
    block_rows = lat_ref.shape[0]
    tok_rows = qn_ref.shape[1]
    offset = lax.axis_index("ep") * tok_rows
    first = block * block_rows

    @pl.when(block == 0)
    def _():
        acc[...] = jnp.zeros_like(acc)
        den[...] = jnp.zeros_like(den)

    @pl.when(first <= offset + tok_rows - 1)
    def _():
        latent = lat_ref[:, :latent_dim]
        rot_key = lat_ref[:, latent_dim:]
        keys = jnp.dot(latent, wk_ref[...], preferred_element_type=jnp.float32)
        values = jnp.dot(latent, wv_ref[...], preferred_element_type=jnp.float32).astype(jnp.bfloat16)
        shape = (tok_rows, block_rows)
        visible = offset + lax.broadcasted_iota(jnp.int32, shape, 0) >= first + lax.broadcasted_iota(
            jnp.int32, shape, 1
        )
        across = (((1,), (1,)), ((), ()))
        for head in range(heads):
            key = keys[:, head * nope_dim : (head + 1) * nope_dim]
            key = rms_norm(key, kg_ref[...]).astype(jnp.bfloat16)
            scores = lax.dot_general(qn_ref[head], key, across, preferred_element_type=jnp.float32)
            scores = scores + lax.dot_general(
                qr_ref[head], rot_key, across, preferred_element_type=jnp.float32
            )
            weights = jnp.where(visible, jnp.exp(scores * scale), 0.0)
            den[head] += jnp.sum(weights, axis=-1, keepdims=True)
            acc[head] += jnp.dot(
                weights.astype(jnp.bfloat16),
                values[:, head * value_dim : (head + 1) * value_dim],
                preferred_element_type=jnp.float32,
            )

    @pl.when(block == pl.num_programs(0) - 1)
    def _():
        for head in range(heads):
            mixed = rms_norm(acc[head] / den[head], og_ref[...])
            out_ref[:, head * value_dim : (head + 1) * value_dim] = mixed.astype(jnp.bfloat16)


def attend(lat_rows, w_key_up, w_value_up, query_nope, query_rope, key_gain, out_gain):
    heads, tok_rows, nope_dim = query_nope.shape
    rope_dim = query_rope.shape[2]
    value_dim = out_gain.shape[0]
    total, width = lat_rows.shape
    block_rows = math.gcd(total, 512)
    whole = pl.BlockSpec(memory_space=VMEM)
    return pl.pallas_call(
        functools.partial(
            attend_kernel, heads, nope_dim, value_dim, width - rope_dim, (nope_dim + rope_dim) ** (-0.5)
        ),
        grid=(total // block_rows,),
        out_shape=jax.ShapeDtypeStruct((tok_rows, heads * value_dim), jnp.bfloat16),
        in_specs=[pl.BlockSpec((block_rows, width), lambda b: (b, 0))] + [whole] * 6,
        out_specs=pl.BlockSpec((tok_rows, heads * value_dim), lambda b: (0, 0)),
        scratch_shapes=[
            VMEM((heads, tok_rows, value_dim), jnp.float32),
            VMEM((heads, tok_rows, 1), jnp.float32),
        ],
        name="attend",
    )(
        lat_rows, w_key_up, w_value_up, query_nope, query_rope,
        key_gain.reshape(1, -1), out_gain.reshape(1, -1),
    )


def on_device(
    queries,
    kv_latent,
    rope_key,
    latent_gain,
    w_key_up,
    w_value_up,
    query_gain,
    key_gain,
    rope_gain,
    out_gain,
    moe_tokens,
    moe_gain,
    routes,
    route_weights,
    w_gate,
    w_up,
    w_down,
):
    quarters = lax.axis_size("tp")
    n_ep = lax.axis_size("ep")
    my_part = lax.axis_index("tp")
    tok_rows = queries.shape[0]
    nope_dim = key_gain.shape[0]
    value_dim = out_gain.shape[0]
    rope_dim = rope_key.shape[1]
    head_count = w_key_up.shape[1] // nope_dim
    positions = lax.axis_index("ep") * tok_rows + jnp.arange(tok_rows, dtype=jnp.int32)
    rot_cos, rot_sin = rope_tables(positions, rope_dim)
    lat_part = tok_rows // quarters

    def mine(values, rows):
        return lax.dynamic_slice_in_dim(values, my_part * rows, rows, 0)

    latent = rms_norm(mine(kv_latent, lat_part).astype(jnp.float32), latent_gain)
    rot_key = rotate(
        rms_norm(mine(rope_key, lat_part).astype(jnp.float32), rope_gain),
        mine(rot_cos, lat_part),
        mine(rot_sin, lat_part),
    )
    lat_own = jnp.concatenate([latent.astype(jnp.bfloat16), rot_key.astype(jnp.bfloat16)], axis=1)

    n_rows, model_dim = moe_tokens.shape
    top_count = routes.shape[1]
    part_rows = n_rows // quarters
    experts = n_ep * w_gate.shape[0]
    capacity = (3 * top_count * part_rows + 2 * experts - 1) // (2 * experts)
    slot_count = experts * capacity
    own_rows = rms_norm(mine(moe_tokens, part_rows).astype(jnp.float32), moe_gain).astype(jnp.bfloat16)
    chosen = mine(routes, part_rows).reshape(part_rows * top_count)
    onehot = (chosen[:, None] == jnp.arange(experts, dtype=jnp.int32)).astype(jnp.float32)
    count = part_rows * top_count
    earlier = (jnp.arange(count)[:, None] > jnp.arange(count)[None, :]).astype(jnp.float32)
    rank = jnp.sum(jnp.dot(earlier, onehot) * onehot, axis=-1).astype(jnp.int32)
    slots = chosen * capacity + rank
    mine_hit = (slots[:, None] == jnp.arange(slot_count, dtype=jnp.int32)).astype(jnp.bfloat16)
    mine_hit = mine_hit.reshape(part_rows, top_count, slot_count)
    outgoing = jnp.einsum(
        "rs,rd->sd", jnp.sum(mine_hit, axis=1), own_rows, preferred_element_type=jnp.float32
    )
    outgoing = outgoing.astype(jnp.bfloat16).reshape(experts, capacity, model_dim)

    arrived, lat_all = spread(outgoing, lat_own, quarters)
    lat_rows = jnp.transpose(lat_all, (2, 1, 0, 3, 4)).reshape(n_ep * tok_rows, lat_own.shape[1])

    shape = arrived.shape
    gate = jnp.einsum("abecd,df->abecf", arrived, w_gate[0], preferred_element_type=jnp.float32)
    upward = jnp.einsum("abecd,df->abecf", arrived, w_up[0], preferred_element_type=jnp.float32)
    hidden = (jax.nn.silu(gate) * upward).astype(jnp.bfloat16)
    partial = jnp.einsum("abecf,fd->aebcd", hidden, w_down[0], preferred_element_type=jnp.float32)
    returned = collect(partial.astype(jnp.bfloat16))

    query = rms_norm(
        queries.astype(jnp.float32).reshape(tok_rows, head_count, nope_dim + rope_dim), query_gain
    )
    query_nope = query[..., :nope_dim].astype(jnp.bfloat16)
    query_rope = rotate(query[..., nope_dim:], rot_cos[:, None, :], rot_sin[:, None, :]).astype(
        jnp.bfloat16
    )
    attended = attend(
        lat_rows,
        w_key_up,
        w_value_up,
        jnp.transpose(query_nope, (1, 0, 2)),
        jnp.transpose(query_rope, (1, 0, 2)),
        key_gain,
        out_gain,
    )

    picked = jnp.einsum(
        "rks,sd->rkd",
        mine_hit,
        returned.reshape(slot_count, model_dim),
        preferred_element_type=jnp.float32,
    )
    own_weights = mine(route_weights, part_rows)
    moe_out = jnp.sum(picked * own_weights[:, :, None], axis=1).astype(jnp.bfloat16)
    return (attended, moe_out)


def solution(mesh):
    return jax.shard_map(
        on_device,
        mesh=mesh,
        in_specs=(
            P("ep", "tp"),
            P("ep", None),
            P("ep", None),
            P(),
            P(None, "tp"),
            P(None, "tp"),
            P(),
            P(),
            P(),
            P(),
            P("ep", None),
            P(),
            P("ep", None),
            P("ep", None),
            P("ep", None, "tp"),
            P("ep", None, "tp"),
            P("ep", "tp", None),
        ),
        out_specs=(P("ep", "tp"), P(("ep", "tp"), None)),
        check_vma=False,
    )
```

time: 216 us -> 126 us (0.58)
  the two profiles are of different devices: /device:TPU:24 before, /device:TPU:6 now
where the time goes in v1:
time: 126 us
  Pallas kernels  92.8 us (74%)
  matrix products  18.9 us (15%)
  other arithmetic  7.22 us (6%)
  local copies, waits for them, and re-layouts  5.99 us (5%)
    pallas_call x1, Pallas kernels, spread(): pl.pallas_call(functools.partial(spread_kernel, n_ep, highs), out_shape=(...  48.3 us
    pallas_call x1, Pallas kernels, collect(): pl.pallas_call(functools.partial(collect_kernel, n_ep, highs), out_shape=...  39.6 us
    dot_general x1, matrix products, on_device(): jnp.einsum('abecd,df->abecf', arrived, w_up[0], preferred_element_type=jn...  5.64 us
    pallas_call x1, Pallas kernels, attend(): pl.pallas_call(functools.partial(attend_kernel, heads, nope_dim, value_di...  4.94 us
    dot_general x1, matrix products, on_device(): jnp.einsum('abecf,fd->aebcd', hidden, w_down[0], preferred_element_type=j...  4.82 us
    dot_general x1, matrix products, on_device(): jnp.einsum('abecd,df->abecf', arrived, w_gate[0], preferred_element_type=...  3.74 us
    transpose x1, local copies, waits for them, and re-layouts, on_device(): jnp.transpose(lat_all, (2, 1, 0, 3, 4))  3.54 us

profile of v1, /device:TPU:6, one launch (start us, length us, event | category | flops | bytes accessed | tf_op | source)
XLA Modules:
  0.0 125.8 jit_solution(7948970193277324940)
XLA Ops:
  0.7 0.8 constant_dynamic-slice_fusion.2
  1.4 0.1 copy.39
  1.5 0.1 eq.51
  1.6 0.1 fusion.16
  1.8 0.1 convert_element_type.59
  2.0 0.8 multiply_add_fusion
  2.8 0.1 fusion.31
  2.9 1.1 fusion.17
  4.0 2.3 %convolution_convert_fusion = bf16[192,2048]{1,0:T(8,128)(2,1)} fusion(bf16[64,192]{1,0:T(8,128)(2,1)S(1)} %fusion.31, f32[2048]{0:T(1024)} %param.28, f32[64]{0:T(128)S(1)} %add_rsqrt_fusion.3, bf16[256,2048]{1,0:T(8,128)(2,1)} %param.27, s32[]{:T(128)S(6)} %select_n.2), kind=kOutput, calls=%fused_computation.9 | convolution fusion | flops 51249152 | bytes 1081604 | tf_op jit(solution)/shard_map/rs,rd->sd/dot_general | solution.py:432
  6.4 0.1 copy.51
  6.5 0.1 fusion.33
  6.6 0.7 fusion.34
  7.4 0.5 multiply_cosine_fusion
  7.9 0.1 subtract_convert_fusion.1
  8.0 1.0 fusion.24
  9.0 0.9 fusion.26
  9.9 0.7 pad_maximum_fusion.lat_ref
  10.7 48.3 %spread.1 = (bf16[2,2,8,24,2048]{4,3,2,1,0:T(8,128)(2,1)}, bf16[2,2,8,64,576]{4,3,2,1,0:T(8,128)(2,1)}) custom-call(bf16[8,24,2048]{2,1,0:T(8,128)(2,1)} %bitcast.51, bf16[64,576]{1,0:T(8,128)(2,1)} %pad_maximum_fusion.lat_ref), custom_call_target="tpu_custom_call" | custom-call | tf_op jit(solution)/shard_map/spread/pallas_call | solution.py:170
  58.9 3.5 %copy.42 = bf16[8,2,2,64,576]{4,3,2,1,0:T(8,128)(2,1)} copy(bf16[8,2,2,64,576]{4,3,0,1,2:T(8,128)(2,1)} %bitcast.52) | data formatting | bytes 4718592 | tf_op jit(solution)/shard_map/transpose | solution.py:438
  62.5 0.1 copy.43
  62.6 0.1 copy.44
  62.9 0.1 multiply_multiply_fusion
  63.0 0.7 fusion.27.qn_ref
  63.7 0.2 subtract_convert_fusion
  63.8 0.8 maximum_bitcast_fusion.qr_ref
  64.6 4.9 %attend.1 = bf16[256,256]{1,0:T(8,128)(2,1)} custom-call(bf16[2048,576]{1,0:T(8,128)(2,1)} %bitcast.50, bf16[512,256]{1,0:T(8,128)(2,1)} %wk_ref.1, bf16[512,256]{1,0:T(8,128)(2,1)} %wv_ref.1, bf16[2,256,128]{2,1,0:T(8,128)(2,1)} %fusion.27.qn_ref, bf16[2,256,64]{2,1,0:T(8,128)(2,1)} %maximum_bitcast_fusion.qr_ref, f32[1,128]{1,0:T(1,128)} %bitcast.56, ...), custom_call_target="tpu_custom_call" | custom-call | tf_op jit(solution)/shard_map/attend/pallas_call | solution.py:356
  69.5 5.6 %fusion.2 = f32[2,2,8,24,896]{4,3,2,1,0:T(8,128)S(1)} fusion(bf16[2,2,8,24,2048]{4,3,2,1,0:T(8,128)(2,1)S(1)} %copy-done.6, bf16[1,2048,896]{2,1,0:T(8,128)(2,1)} %param.32), kind=kOutput, calls=%fused_computation.2 | convolution fusion | flops 2818572288 | bytes 9568256 | tf_op jit(solution)/shard_map/abecd,df->abecf/dot_general | solution.py:442
  75.2 3.7 %multiply_convert_fusion = bf16[2,2,8,24,896]{4,3,2,1,0:T(8,128)(2,1)S(1)} fusion(f32[2,2,8,24,896]{4,3,2,1,0:T(8,128)S(1)} %fusion.2, bf16[2,2,8,24,2048]{4,3,2,1,0:T(8,128)(2,1)S(1)} %copy-done.6, bf16[1,2048,896]{2,1,0:T(8,128)(2,1)S(1)} %copy-done.4), kind=kOutput, calls=%fused_computation.8 | convolution fusion | flops 2822701056 | bytes 10944512 | tf_op jit(solution)/shard_map/abecd,df->abecf/dot_general | solution.py:441
  79.0 4.8 %fusion.9.part_ref = bf16[2,8,2,24,2048]{4,3,2,1,0:T(8,128)(2,1)} fusion(bf16[1,896,2048]{2,1,0:T(8,128)(2,1)S(1)} %copy-done.5, bf16[2,2,8,24,896]{4,3,2,1,0:T(8,128)(2,1)S(1)} %multiply_convert_fusion), kind=kOutput, calls=%fused_computation.7 | convolution fusion | flops 2820145152 | bytes 8192000 | tf_op jit(solution)/shard_map/abecf,fd->aebcd/dot_general | solution.py:444
  83.8 39.6 %collect.1 = bf16[8,24,2048]{2,1,0:T(8,128)(2,1)} custom-call(bf16[2,8,2,24,2048]{4,3,2,1,0:T(8,128)(2,1)} %fusion.9.part_ref), custom_call_target="tpu_custom_call" | custom-call | tf_op jit(solution)/shard_map/collect/pallas_call | solution.py:277
  123.4 0.1 constant_dynamic-slice_fusion
  123.5 2.3 %fusion.15 = bf16[64,2048]{1,0:T(8,128)(2,1)} fusion(bf16[192,2048,1]{1,0,2:T(8,128)(2,1)} %bitcast.55, f32[64,2]{0,1:T(2,128)S(1)} %constant_dynamic-slice_fusion, s32[64,2]{0,1:T(2,128)S(1)} %multiply_add_fusion), kind=kOutput, calls=%fused_computation.12 | convolution fusion | flops 101081088 | bytes 1049600 | tf_op jit(solution)/shard_map/rks,sd->rkd/dot_general | solution.py:464
  (24 shorter events, 0.3 us)
Async XLA Ops:
  0.6 5.7 %copy-start = (bf16[256,64]{0,1:T(8,128)(2,1)S(1)}, bf16[256,64]{0,1:T(8,128)(2,1)}, u32[]{:S(2)}) copy-start(bf16[256,64]{0,1:T(8,128)(2,1)} %param.19) | copy-start | bytes 98308
  9.9 52.5 %copy-start.1 = (bf16[256,384]{1,0:T(8,128)(2,1)S(1)}, bf16[256,384]{1,0:T(8,128)(2,1)}, u32[]{:S(2)}) copy-start(bf16[256,384]{1,0:T(8,128)(2,1)} %param.17) | copy-start | bytes 589828
  58.9 3.9 %copy-start.2 = (f32[192]{0:T(256)S(1)}, f32[192]{0:T(256)}, u32[]{:S(2)}) copy-start(f32[192]{0:T(256)} %param.23) | copy-start | bytes 2308
  63.0 6.5 %copy-start.6 = (bf16[2,2,8,24,2048]{4,3,2,1,0:T(8,128)(2,1)S(1)}, bf16[2,2,8,24,2048]{4,3,2,1,0:T(8,128)(2,1)}, u32[]{:S(2)}) copy-start(bf16[2,2,8,24,2048]{4,3,2,1,0:T(8,128)(2,1)} %get-tuple-element.5) | copy-start | bytes 9437188
  69.5 5.7 %copy-start.4 = (bf16[1,2048,896]{2,1,0:T(8,128)(2,1)S(1)}, bf16[1,2048,896]{2,1,0:T(8,128)(2,1)}, u32[]{:S(2)}) copy-start(bf16[1,2048,896]{2,1,0:T(8,128)(2,1)} %param.31) | copy-start | bytes 11010052
  75.2 3.8 %copy-start.5 = (bf16[1,896,2048]{2,1,0:T(8,128)(2,1)S(1)}, bf16[1,896,2048]{2,1,0:T(8,128)(2,1)}, u32[]{:S(2)}) copy-start(bf16[1,896,2048]{2,1,0:T(8,128)(2,1)} %param.33) | copy-start | bytes 11010052
  83.8 39.6 %copy-start.3 = (f32[256,2]{0,1:T(2,128)S(1)}, f32[256,2]{0,1:T(2,128)}, u32[]{:S(2)}) copy-start(f32[256,2]{0,1:T(2,128)} %param.30) | copy-start | bytes 6148

commit v2 on v1

--- a/solution.py
+++ b/solution.py
@@ -71,11 +71,11 @@
     partner = (me, high * 2 + 1 - low)
     greet(me, quarter, n_ep, highs)
     payloads = (
-        (lambda j: rows_ref.at[j], arrived),
-        (lambda j: lat_ref, lat_all),
+        (lambda j: rows_ref.at[j], lambda c, h, j: arrived.at[c, h, j]),
+        (lambda j: lat_ref, lambda c, h, j: lat_all.at[j, h, c]),
     )
     own = [
-        pltpu.make_async_copy(outgoing(me), into.at[low, high, me], own_sem.at[p])
+        pltpu.make_async_copy(outgoing(me), into(low, high, me), own_sem.at[p])
         for p, (outgoing, into) in enumerate(payloads)
     ]
     for copy in own:
@@ -85,20 +85,20 @@
         outgoing, into = payloads[p]
         j = lax.rem(me + step, n_ep)
         return remote(
-            outgoing(j), into.at[low, high, me], ep_send.at[p, step], ep_recv.at[p, step], (j, quarter)
+            outgoing(j), into(low, high, me), ep_send.at[p, step], ep_recv.at[p, step], (j, quarter)
         )
 
     def ep_arrival(p, step):
         outgoing, into = payloads[p]
         j = lax.rem(me + n_ep - step, n_ep)
         return remote(
-            outgoing(me), into.at[low, high, j], ep_send.at[p, step], ep_recv.at[p, step], (j, quarter)
+            outgoing(me), into(low, high, j), ep_send.at[p, step], ep_recv.at[p, step], (j, quarter)
         )
 
     def high_copy(p, step, hop):
         into = payloads[p][1]
         j = lax.rem(me + n_ep - step, n_ep)
-        block = into.at[low, high, j]
+        block = into(low, high, j)
         return remote(
             block, block, high_send.at[p, hop, step], high_recv.at[p, hop, step],
             (me, lax.rem(high + hop, highs) * 2 + low),
@@ -107,7 +107,7 @@
     def high_arrival(p, step, hop):
         into = payloads[p][1]
         j = lax.rem(me + n_ep - step, n_ep)
-        block = into.at[low, lax.rem(high + highs - hop, highs), j]
+        block = into(low, lax.rem(high + highs - hop, highs), j)
         return remote(
             block, block, high_send.at[p, hop, step], high_recv.at[p, hop, step],
             (me, lax.rem(high + hop, highs) * 2 + low),
@@ -116,7 +116,7 @@
     def low_copy(p, step, hop, side):
         into = payloads[p][1]
         j = lax.rem(me + n_ep - step, n_ep)
-        block = into.at[side, lax.rem(high + highs - hop, highs), j]
+        block = into(side, lax.rem(high + highs - hop, highs), j)
         return remote(block, block, low_send.at[p, hop, step], low_recv.at[p, hop, step], partner)
 
     def start_ep(step, carry, p):
@@ -148,19 +148,20 @@
         ep_copy(p, step).wait_send()
         return carry
 
+    sent, came = (n_ep, n_ep - me), (n_ep, me + 1)
     for p in range(2):
-        lax.fori_loop(1, n_ep, functools.partial(start_ep, p=p), 0)
+        lax.fori_loop(1, sent[p], functools.partial(start_ep, p=p), 0)
     for p in range(2):
         own[p].wait()
         for hop in range(1, highs):
             high_copy(p, 0, hop).start()
         low_copy(p, 0, 0, low).start()
-        lax.fori_loop(1, n_ep, functools.partial(forward, p=p), 0)
+        lax.fori_loop(1, came[p], functools.partial(forward, p=p), 0)
     for p in range(2):
-        lax.fori_loop(0, n_ep, functools.partial(forward_low, p=p), 0)
+        lax.fori_loop(0, came[p], functools.partial(forward_low, p=p), 0)
     for p in range(2):
-        lax.fori_loop(0, n_ep, functools.partial(finish, p=p), 0)
-        lax.fori_loop(1, n_ep, functools.partial(finish_ep, p=p), 0)
+        lax.fori_loop(0, came[p], functools.partial(finish, p=p), 0)
+        lax.fori_loop(1, sent[p], functools.partial(finish_ep, p=p), 0)
 
 
 def spread(rows, lat, quarters):
@@ -171,7 +172,7 @@
         functools.partial(spread_kernel, n_ep, highs),
         out_shape=(
             jax.ShapeDtypeStruct((2, highs, n_ep, cap, model_dim), rows.dtype),
-            jax.ShapeDtypeStruct((2, highs, n_ep) + lat.shape, lat.dtype),
+            jax.ShapeDtypeStruct((n_ep, highs, 2) + lat.shape, lat.dtype),
         ),
         in_specs=[pl.BlockSpec(memory_space=VMEM)] * 2,
         out_specs=(pl.BlockSpec(memory_space=VMEM),) * 2,
@@ -351,7 +352,7 @@
     rope_dim = query_rope.shape[2]
     value_dim = out_gain.shape[0]
     total, width = lat_rows.shape
-    block_rows = math.gcd(total, 512)
+    block_rows = math.gcd(total, tok_rows)
     whole = pl.BlockSpec(memory_space=VMEM)
     return pl.pallas_call(
         functools.partial(
@@ -435,7 +436,7 @@
     outgoing = outgoing.astype(jnp.bfloat16).reshape(experts, capacity, model_dim)
 
     arrived, lat_all = spread(outgoing, lat_own, quarters)
-    lat_rows = jnp.transpose(lat_all, (2, 1, 0, 3, 4)).reshape(n_ep * tok_rows, lat_own.shape[1])
+    lat_rows = lat_all.reshape(n_ep * tok_rows, lat_own.shape[1])
 
     shape = arrived.shape
     gate = jnp.einsum("abecd,df->abecf", arrived, w_gate[0], preferred_element_type=jnp.float32)

time: 126 us -> 127 us (level)
  local copies, waits for them, and re-layouts: 5.99 us -> 2.49 us
  Pallas kernels: 92.8 us -> 95.6 us
    pallas_call x1, Pallas kernels: 39.6 us -> 51.7 us  [collect(): pl.pallas_call(functools.partial(collect_kernel, n_ep, highs), out_shape=...]
    pallas_call x1, Pallas kernels: 48.3 us -> 36.6 us  [spread(): pl.pallas_call(functools.partial(spread_kernel, n_ep, highs), out_shape=(...]
    transpose x1 -> x0, local copies, waits for them, and re-layouts: 3.54 us -> none  [on_device(): jnp.transpose(lat_all, (2, 1, 0, 3, 4))]
    pallas_call x1, Pallas kernels: 4.94 us -> 7.24 us  [attend(): pl.pallas_call(functools.partial(attend_kernel, heads, nope_dim, value_di...]
where the time goes in v2:
time: 127 us; the launch traced here: 126 us
  Pallas kernels  95.6 us (75%)
  matrix products  19.8 us (16%)
  other arithmetic  7.22 us (6%)
  local copies, waits for them, and re-layouts  2.49 us (2%)
    pallas_call x1, Pallas kernels, collect(): pl.pallas_call(functools.partial(collect_kernel, n_ep, highs), out_shape=...  51.7 us
    pallas_call x1, Pallas kernels, spread(): pl.pallas_call(functools.partial(spread_kernel, n_ep, highs), out_shape=(...  36.6 us
    pallas_call x1, Pallas kernels, attend(): pl.pallas_call(functools.partial(attend_kernel, heads, nope_dim, value_di...  7.24 us
    dot_general x1, matrix products, on_device(): jnp.einsum('abecd,df->abecf', arrived, w_up[0], preferred_element_type=jn...  6.54 us
    dot_general x1, matrix products, on_device(): jnp.einsum('abecf,fd->aebcd', hidden, w_down[0], preferred_element_type=j...  4.83 us
    dot_general x1, matrix products, on_device(): jnp.einsum('abecd,df->abecf', arrived, w_gate[0], preferred_element_type=...  3.73 us

profile of v2, /device:TPU:6, one launch (start us, length us, event | category | flops | bytes accessed | tf_op | source)
XLA Modules:
  0.0 126.0 jit_solution(2571608717630786742)
XLA Ops:
  0.7 0.8 constant_dynamic-slice_fusion.2
  1.5 0.1 copy.36
  1.6 0.1 eq.51
  1.7 0.1 fusion.16
  1.9 0.1 convert_element_type.59
  2.1 0.8 multiply_add_fusion
  2.9 0.1 fusion.31
  3.0 1.1 fusion.17
  4.1 2.3 %convolution_convert_fusion = bf16[192,2048]{1,0:T(8,128)(2,1)} fusion(bf16[64,192]{1,0:T(8,128)(2,1)S(1)} %fusion.31, f32[2048]{0:T(1024)} %param.28, f32[64]{0:T(128)S(1)} %add_rsqrt_fusion.3, bf16[256,2048]{1,0:T(8,128)(2,1)} %param.27, s32[]{:T(128)S(6)} %select_n.2), kind=kOutput, calls=%fused_computation.9 | convolution fusion | flops 51249152 | bytes 1081604 | tf_op jit(solution)/shard_map/rs,rd->sd/dot_general | solution.py:433
  6.4 0.1 constant_dynamic-slice_fusion.1
  6.5 0.1 copy.47
  6.5 0.1 fusion.33
  6.7 0.7 fusion.34
  7.4 0.5 multiply_cosine_fusion
  8.0 0.1 subtract_convert_fusion.1
  8.1 1.0 fusion.24
  9.0 0.9 fusion.26
  10.0 0.7 pad_maximum_fusion.lat_ref
  10.7 36.6 %spread.1 = (bf16[2,2,8,24,2048]{4,3,2,1,0:T(8,128)(2,1)}, bf16[8,2,2,64,576]{4,3,2,1,0:T(8,128)(2,1)}) custom-call(bf16[8,24,2048]{2,1,0:T(8,128)(2,1)} %bitcast.49, bf16[64,576]{1,0:T(8,128)(2,1)} %pad_maximum_fusion.lat_ref), custom_call_target="tpu_custom_call" | custom-call | tf_op jit(solution)/shard_map/spread/pallas_call | solution.py:171
  47.4 0.1 copy.39
  47.5 0.1 copy.40
  47.8 0.1 multiply_multiply_fusion
  47.9 0.7 fusion.27.qn_ref
  48.6 0.2 subtract_convert_fusion
  48.7 0.8 maximum_bitcast_fusion.qr_ref
  49.5 7.2 %attend.1 = bf16[256,256]{1,0:T(8,128)(2,1)} custom-call(bf16[2048,576]{1,0:T(8,128)(2,1)} %bitcast.50, bf16[512,256]{1,0:T(8,128)(2,1)} %wk_ref.1, bf16[512,256]{1,0:T(8,128)(2,1)} %wv_ref.1, bf16[2,256,128]{2,1,0:T(8,128)(2,1)} %fusion.27.qn_ref, bf16[2,256,64]{2,1,0:T(8,128)(2,1)} %maximum_bitcast_fusion.qr_ref, f32[1,128]{1,0:T(1,128)} %bitcast.54, ...), custom_call_target="tpu_custom_call" | custom-call | tf_op jit(solution)/shard_map/attend/pallas_call | solution.py:357
  56.7 6.5 %fusion.2 = f32[2,2,8,24,896]{4,3,2,1,0:T(8,128)S(1)} fusion(bf16[2,2,8,24,2048]{4,3,2,1,0:T(8,128)(2,1)} %get-tuple-element.5, bf16[1,2048,896]{2,1,0:T(8,128)(2,1)} %param.32), kind=kOutput, calls=%fused_computation.2 | convolution fusion | flops 2818572288 | bytes 9568256 | tf_op jit(solution)/shard_map/abecd,df->abecf/dot_general | solution.py:443
  63.3 3.7 %multiply_convert_fusion = bf16[2,2,8,24,896]{4,3,2,1,0:T(8,128)(2,1)S(1)} fusion(f32[2,2,8,24,896]{4,3,2,1,0:T(8,128)S(1)} %fusion.2, bf16[2,2,8,24,2048]{4,3,2,1,0:T(8,128)(2,1)S(1)} %copy-done.6, bf16[1,2048,896]{2,1,0:T(8,128)(2,1)S(1)} %copy-done.4), kind=kOutput, calls=%fused_computation.8 | convolution fusion | flops 2822701056 | bytes 10944512 | tf_op jit(solution)/shard_map/abecd,df->abecf/dot_general | solution.py:442
  67.1 4.8 %fusion.9.part_ref = bf16[2,8,2,24,2048]{4,3,2,1,0:T(8,128)(2,1)} fusion(bf16[1,896,2048]{2,1,0:T(8,128)(2,1)S(1)} %copy-done.5, bf16[2,2,8,24,896]{4,3,2,1,0:T(8,128)(2,1)S(1)} %multiply_convert_fusion), kind=kOutput, calls=%fused_computation.7 | convolution fusion | flops 2820145152 | bytes 8192000 | tf_op jit(solution)/shard_map/abecf,fd->aebcd/dot_general | solution.py:445
  71.9 51.7 %collect.1 = bf16[8,24,2048]{2,1,0:T(8,128)(2,1)} custom-call(bf16[2,8,2,24,2048]{4,3,2,1,0:T(8,128)(2,1)} %fusion.9.part_ref), custom_call_target="tpu_custom_call" | custom-call | tf_op jit(solution)/shard_map/collect/pallas_call | solution.py:278
  123.7 0.1 constant_dynamic-slice_fusion
  123.7 2.3 %fusion.15 = bf16[64,2048]{1,0:T(8,128)(2,1)} fusion(bf16[192,2048,1]{1,0,2:T(8,128)(2,1)} %bitcast.53, f32[64,2]{0,1:T(2,128)S(1)} %constant_dynamic-slice_fusion, s32[64,2]{0,1:T(2,128)S(1)} %multiply_add_fusion), kind=kOutput, calls=%fused_computation.12 | convolution fusion | flops 101081088 | bytes 1049600 | tf_op jit(solution)/shard_map/rks,sd->rkd/dot_general | solution.py:465
  (23 shorter events, 0.2 us)
Async XLA Ops:
  0.6 5.7 %copy-start = (bf16[256,64]{0,1:T(8,128)(2,1)S(1)}, bf16[256,64]{0,1:T(8,128)(2,1)}, u32[]{:S(2)}) copy-start(bf16[256,64]{0,1:T(8,128)(2,1)} %param.19) | copy-start | bytes 98308
  0.6 46.7 %copy-start.1 = (bf16[256,384]{1,0:T(8,128)(2,1)S(1)}, bf16[256,384]{1,0:T(8,128)(2,1)}, u32[]{:S(2)}) copy-start(bf16[256,384]{1,0:T(8,128)(2,1)} %param.17) | copy-start | bytes 589828
  0.7 47.1 %copy-start.2 = (f32[192]{0:T(256)S(1)}, f32[192]{0:T(256)}, u32[]{:S(2)}) copy-start(f32[192]{0:T(256)} %param.23) | copy-start | bytes 2308
  56.7 6.6 %copy-start.4 = (bf16[1,2048,896]{2,1,0:T(8,128)(2,1)S(1)}, bf16[1,2048,896]{2,1,0:T(8,128)(2,1)}, u32[]{:S(2)}) copy-start(bf16[1,2048,896]{2,1,0:T(8,128)(2,1)} %param.31) | copy-start | bytes 11010052
  56.7 6.6 %copy-start.6 = (bf16[2,2,8,24,2048]{4,3,2,1,0:T(8,128)(2,1)S(1)}, bf16[2,2,8,24,2048]{4,3,2,1,0:T(8,128)(2,1)}, u32[]{:S(2)}) copy-start(bf16[2,2,8,24,2048]{4,3,2,1,0:T(8,128)(2,1)} %get-tuple-element.5) | copy-start | bytes 9437188
  63.3 3.8 %copy-start.5 = (bf16[1,896,2048]{2,1,0:T(8,128)(2,1)S(1)}, bf16[1,896,2048]{2,1,0:T(8,128)(2,1)}, u32[]{:S(2)}) copy-start(bf16[1,896,2048]{2,1,0:T(8,128)(2,1)} %param.33) | copy-start | bytes 11010052
  71.9 51.8 %copy-start.3 = (f32[256,2]{0,1:T(2,128)S(1)}, f32[256,2]{0,1:T(2,128)}, u32[]{:S(2)}) copy-start(f32[256,2]{0,1:T(2,128)} %param.30) | copy-start | bytes 6148
